TPU v7x, 32 devices: a whole 2x2x4 slice. The times are simulated.
32 devices in a mesh: gr: 2 (over x), fs: 8 (over z, y), tp: 2 (over core).
Axes of the slice: x: 2, y: 2, z: 4, core: 2. Of those that a mesh axis runs over, the one named last changes fastest.
Arguments:
- tokens: bfloat16 [4096, 2048], P(('gr', 'fs', 'tp')), may hold values from -6 to 6
- norm_gain: float32 [2048], P(('gr', 'fs')), may hold values from 0.1 to 1.9
- up_weight: float32 [2048, 8192], P(('gr', 'fs'), 'tp'), may hold values from -0.125 to 0.125
- down_weight: float32 [8192, 2048], P(('gr', 'fs'), 'tp'), may hold values from -0.0625 to 0.0625
Outputs:
- served: bfloat16 [4096, 2048], P(('gr', 'fs', 'tp'))
- serve_up: bfloat16 [2048, 8192], P(None, 'fs')
- serve_down: bfloat16 [8192, 2048], P('fs')
All inputs are finite; a program needn't handle non-finite values.
Results may differ from a plain program's by a relative error of at most 0.017.
Values may be sent and summed in bfloat16 or wider, within the bound.
A program may use at most 64 MiB of HBM per device.

v0:
```python
import jax
import jax.numpy as jnp
from jax import lax
from jax.sharding import PartitionSpec as P


def body(tokens, norm_gain, up_weight, down_weight):
    groups = lax.axis_size("gr")
    shards = lax.axis_size("fs")
    segment = down_weight.shape[0]
    own_rows = up_weight.shape[0]
    up_local = (norm_gain[:, None] * up_weight).astype(jnp.bfloat16)
    down_local = down_weight.astype(jnp.bfloat16)
    up_cols, down_cols = (
        lax.all_gather(up_local, "tp", axis=1, tiled=True),
        lax.all_gather(down_local, "tp", axis=1, tiled=True),
    )
    width = up_cols.shape[1]
    up_sorted = (
        up_cols.reshape(own_rows, groups, shards, segment)
        .transpose(0, 2, 1, 3)
        .reshape(own_rows, width)
    )
    up_mine = lax.all_to_all(up_sorted, "fs", split_axis=1, concat_axis=0, tiled=True)
    serve_up, serve_down = (
        lax.all_gather(up_mine, "gr", axis=0, tiled=True),
        lax.all_gather(down_cols, "gr", axis=0, tiled=True),
    )
    values = tokens.astype(jnp.float32)
    normed = (values * lax.rsqrt(jnp.mean(values * values, axis=1, keepdims=True) + 1e-06)).astype(
        jnp.bfloat16
    )
    product = jnp.dot(
        lax.all_gather(normed, "fs", axis=0, tiled=True),
        serve_up,
        preferred_element_type=jnp.float32,
    )
    hidden = jnp.square(jax.nn.relu(product)).astype(jnp.bfloat16)
    part = jnp.dot(hidden, serve_down, preferred_element_type=jnp.float32).astype(jnp.bfloat16)
    part = lax.optimization_barrier(part)
    summed = lax.psum_scatter(
        part.astype(jnp.float32).astype(jnp.bfloat16), "fs", scatter_dimension=0, tiled=True
    )
    return (summed, serve_up, serve_down)


def solution(mesh):
    return jax.shard_map(
        body,
        mesh=mesh,
        in_specs=(
            P(("gr", "fs", "tp"), None),
            P(("gr", "fs")),
            P(("gr", "fs"), "tp"),
            P(("gr", "fs"), "tp"),
        ),
        out_specs=(P(("gr", "fs", "tp"), None), P(None, "fs"), P("fs", None)),
        check_vma=False,
    )
```

profile of v0, /device:TPU:0, one launch (start us, length us, event | category | flops | bytes accessed | tf_op | source)
XLA Modules:
  0.0 345.5 jit_solution(10217558467831381124)
XLA Ops:
  7.2 0.0 all-gather.12.cloned.1.call-start
  7.2 2.9 convert_element_type.24
  10.1 0.0 all-gather.12.cloned.1.call-update
  10.1 0.0 all-gather.8.cloned.1.call-start
  10.2 0.0 copy-done.1
  10.2 0.0 copy-done.3
  10.2 1.2 multiply_convert_fusion.1
  11.4 0.0 all-gather.8.cloned.1.call-update
  11.4 0.0 all-gather.14.cloned.1.call-start
  11.4 12.1 %all-gather.12.cloned.1.call-done = bf16[512,2048]{1,0:T(8,128)(2,1)} async-done(((bf16[512,1024]{1,0:T(8,128)(2,1)}), bf16[512,2048]{1,0:T(8,128)(2,1)}) %all-gather.12.cloned.1.call-update) | async-done | bytes 2097168 | tf_op jit(solution)/shard_map/all_gather | solution.py:16
  23.6 0.0 all-gather.14.cloned.1.call-update
  23.6 0.0 all-gather.6.cloned.1.call-start
  23.6 0.0 copy-done.2
  23.7 0.2 fusion
  23.9 1.0 fusion.1
  24.8 0.0 all-gather.6.cloned.1.call-update
  24.8 0.0 all-gather.10.cloned.1.call-start
  24.9 12.6 %all-gather.8.cloned.1.call-done = bf16[128,8192]{1,0:T(8,128)(2,1)} async-done(((bf16[128,4096]{1,0:T(8,128)(2,1)}), bf16[128,8192]{1,0:T(8,128)(2,1)}) %all-gather.8.cloned.1.call-update) | async-done | bytes 2097168 | tf_op jit(solution)/shard_map/all_gather | solution.py:15
  37.5 2.4 copy.8
  39.9 1.6 copy.7
  41.5 2.7 all_to_all.14
  44.2 54.5 %all_to_all.19 = bf16[128,8,1024]{2,0,1:T(8,128)(2,1)} all-to-all(bf16[128,8,1024]{2,0,1:T(8,128)(2,1)} %all_to_all.14), channel_id=1, replica_groups=mesh['gr'=2,'fs'=8,'tp'=2] {'fs'}, dimensions={1} | all-to-all | bytes 4194304 | tf_op jit(solution)/shard_map/all_to_all | solution.py:24
  98.8 0.0 all-gather.10.cloned.1.call-update
  98.8 0.0 reduce-scatter.2.cloned.1.call-start
  98.8 0.0 all-gather.14.cloned.1.call-done
  98.9 73.5 %all-gather.6.cloned.1.call-done = bf16[1024,2048]{1,0:T(8,128)(2,1)} async-done(((bf16[128,2048]{1,0:T(8,128)(2,1)}), bf16[1024,2048]{1,0:T(8,128)(2,1)}) %all-gather.6.cloned.1.call-update) | async-done | bytes 4194320 | tf_op jit(solution)/shard_map/all_gather | solution.py:34
  172.3 56.7 %all-gather.10.cloned.1.call-done = bf16[2048,1024]{1,0:T(8,128)(2,1)} async-done(((bf16[1024,1024]{1,0:T(8,128)(2,1)}), bf16[2048,1024]{1,0:T(8,128)(2,1)}) %all-gather.10.cloned.1.call-update) | async-done | bytes 4194320 | tf_op jit(solution)/shard_map/all_gather | solution.py:26
  229.0 14.4 %convolution_convert_fusion = bf16[1024,2048]{1,0:T(8,128)(2,1)} fusion(bf16[1024,2048]{1,0:T(8,128)(2,1)} %all-gather.14.cloned.1.call-done, bf16[1024,2048]{1,0:T(8,128)(2,1)} %all-gather.6.cloned.1.call-done, bf16[2048,1024]{1,0:T(8,128)(2,1)} %all-gather.10.cloned.1.call-done), kind=kOutput, calls=%fused_computation.1 | convolution fusion | flops 8595177472 | bytes 16777216 | tf_op jit(solution)/shard_map/dot_general | solution.py:39
  243.4 0.0 reduce-scatter.2.cloned.1.call-update
  243.4 88.5 %reduce-scatter.2.cloned.1.call-done = bf16[128,2048]{1,0:T(8,128)(2,1)} async-done(((bf16[1024,2048]{1,0:T(8,128)(2,1)}), bf16[128,2048]{1,0:T(8,128)(2,1)}) %reduce-scatter.2.cloned.1.call-update) | async-done | bytes 524304 | tf_op jit(solution)/shard_map/reduce_scatter | solution.py:41
  331.9 4.8 %copy.11 = bf16[2048,1024]{1,0:T(8,128)(2,1)} copy(bf16[2048,1024]{1,0:T(8,128)(2,1)} %all-gather.10.cloned.1.call-done) | data formatting | bytes 8388608
  336.7 2.0 copy.12
  (6 shorter events, 0.0 us)
Async XLA Ops:
  7.2 3.0 copy-start.1
  7.2 3.0 copy-start.3
  7.2 16.4 %all-gather.12.cloned.1.call-start = ((), (), s32[]{:S(2)}) async-start(), calls=%async_computation.5 | async-start | bytes 3145728 | tf_op jit(solution)/shard_map/all_gather | solution.py:16
  10.1 13.6 %copy-start.2 = (bf16[128,2048]{1,0:T(8,128)(2,1)S(1)}, bf16[128,2048]{1,0:T(8,128)(2,1)}, u32[]{:S(2)}) copy-start(bf16[128,2048]{1,0:T(8,128)(2,1)} %param.4) | copy-start | bytes 1572868
  10.1 27.4 %all-gather.8.cloned.1.call-start = ((), (), s32[]{:S(2)}) async-start(), calls=%async_computation.3 | async-start | bytes 3145728 | tf_op jit(solution)/shard_map/all_gather | solution.py:15
  11.4 87.5 %all-gather.14.cloned.1.call-start = ((), (), s32[]{:S(2)}) async-start(), calls=%async_computation.6 | async-start | bytes 6291456 | tf_op jit(solution)/shard_map/all_gather | solution.py:27
  23.6 148.7 %all-gather.6.cloned.1.call-start = ((), (), s32[]{:S(2)}) async-start(), calls=%async_computation.2 | async-start | bytes 4718592 | tf_op jit(solution)/shard_map/all_gather | solution.py:34
  24.8 204.2 %all-gather.10.cloned.1.call-start = ((), (), s32[]{:S(2)}) async-start(), calls=%async_computation.4 | async-start | bytes 6291456 | tf_op jit(solution)/shard_map/all_gather | solution.py:26
  98.8 233.1 %reduce-scatter.2.cloned.1.call-start = ((), (), s32[]{:S(2)}) async-start(), calls=%async_computation.7 | async-start | bytes 4718592 | tf_op jit(solution)/shard_map/reduce_scatter | solution.py:41
  331.9 4.8 %copy-start = (bf16[1024,2048]{1,0:T(8,128)(2,1)S(1)}, bf16[1024,2048]{1,0:T(8,128)(2,1)}, u32[]{:S(2)}) copy-start(bf16[1024,2048]{1,0:T(8,128)(2,1)} %all-gather.14.cloned.1.call-done) | copy-start | bytes 12582916
Sparse Core Ops, SparseCore 0:
  10.2 13.2 all-gather.11
  25.7 11.7 all-gather.7
  39.0 57.8 all-gather.13
  99.5 72.7 all-gather.5
  173.7 55.2 all-gather.9
  243.5 88.2 reduce-scatter.1
where the time goes:
time: 346 us
  waiting for transfers between devices  243 us (70%)
  blocking collectives  54.5 us (16%)
  matrix products  14.4 us (4%)
  between operations  14.2 us (4%)
  local copies, waits for them, and re-layouts  13.6 us (4%)
  other arithmetic  5.2 us (2%)
    reduce_scatter x1, waiting for transfers between devices, body(): lax.psum_scatter(part.astype(jnp.float32).astype(jnp.bfloat16), 'fs', sca...  88.5 us
    all_gather x1, waiting for transfers between devices, body(): lax.all_gather(normed, 'fs', axis=0, tiled=True)  73.5 us
    all_gather x1, waiting for transfers between devices, body(): lax.all_gather(up_mine, 'gr', axis=0, tiled=True)  56.7 us
    all_to_all x1, blocking collectives, body(): lax.all_to_all(up_sorted, 'fs', split_axis=1, concat_axis=0, tiled=True)  54.5 us
    dot_general x1, matrix products, body(): jnp.dot(hidden, serve_down, preferred_element_type=jnp.float32)  14.4 us
    all_gather x1, waiting for transfers between devices, body(): lax.all_gather(up_local, 'tp', axis=1, tiled=True)  12.6 us
    all_gather x1, waiting for transfers between devices, body(): lax.all_gather(down_local, 'tp', axis=1, tiled=True)  12.1 us
    unnamed x11, local copies, waits for them, and re-layouts  9.26 us
  transfers between devices with their start and end apart: 6, of which 5 were waited for; matrix products, arithmetic and copies ran while one was open for 2% of the time, Pallas kernels for 0%

commit v1 on v0

--- a/solution.py
+++ b/solution.py
@@ -2,6 +2,13 @@
 import jax.numpy as jnp
 from jax import lax
 from jax.sharding import PartitionSpec as P
+
+
+def all_by_exchange(value, axis, along):
+    devices = lax.axis_size(axis)
+    blocks = jnp.stack([value for _ in range(devices)])
+    blocks = lax.all_to_all(blocks, axis, split_axis=0, concat_axis=0)
+    return jnp.concatenate(blocks, axis=along)
 
 
 def body(tokens, norm_gain, up_weight, down_weight):
@@ -23,7 +30,7 @@
     )
     up_mine = lax.all_to_all(up_sorted, "fs", split_axis=1, concat_axis=0, tiled=True)
     serve_up, serve_down = (
-        lax.all_gather(up_mine, "gr", axis=0, tiled=True),
+        all_by_exchange(up_mine, "gr", 0),
         lax.all_gather(down_cols, "gr", axis=0, tiled=True),
     )
     values = tokens.astype(jnp.float32)

time: 346 us -> 287 us (0.83)
  waiting for transfers between devices: 243 us -> 178 us
  starting transfers between devices: 0.24 us -> 5.84 us
    all_gather x1 -> x0, waiting for transfers between devices: 56.7 us -> none  [body(): lax.all_gather(up_mine, 'gr', axis=0, tiled=True)]
    all_gather x1, waiting for transfers between devices: 73.5 us -> 67.8 us  [body(): lax.all_gather(normed, 'fs', axis=0, tiled=True)]
    all_to_all x0 -> x1, starting transfers between devices: none -> 5.64 us  [all_by_exchange(): blocks = lax.all_to_all(blocks, axis, split_axis=0, concat_axis=0)]
    unnamed x11 -> x9, local copies, waits for them, and re-layouts: 9.26 us -> 8.75 us
  transfers between devices with their start and end apart: 6 -> 6, of which waited for: 5 -> 4; matrix products, arithmetic and copies ran while one was open for 2% -> 4% of each run, Pallas kernels for 0% -> 0%
where the time goes in v1:
time: 287 us
  waiting for transfers between devices  178 us (62%)
  blocking collectives  54.3 us (19%)
  matrix products  14.4 us (5%)
  between operations  13.9 us (5%)
  local copies, waits for them, and re-layouts  13.4 us (5%)
  other arithmetic  7.33 us (3%)
  starting transfers between devices  5.84 us (2%)
    reduce_scatter x1, waiting for transfers between devices, body(): lax.psum_scatter(part.astype(jnp.float32).astype(jnp.bfloat16), 'fs', sca...  87 us
    all_gather x1, waiting for transfers between devices, body(): lax.all_gather(normed, 'fs', axis=0, tiled=True)  67.8 us
    all_to_all x1, blocking collectives, body(): lax.all_to_all(up_sorted, 'fs', split_axis=1, concat_axis=0, tiled=True)  54.3 us
    dot_general x1, matrix products, body(): jnp.dot(hidden, serve_down, preferred_element_type=jnp.float32)  14.4 us
    all_gather x1, waiting for transfers between devices, body(): lax.all_gather(up_local, 'tp', axis=1, tiled=True)  12.6 us
    all_gather x1, waiting for transfers between devices, body(): lax.all_gather(down_local, 'tp', axis=1, tiled=True)  10.3 us
    unnamed x9, local copies, waits for them, and re-layouts  8.75 us
  transfers between devices with their start and end apart: 6, of which 4 were waited for; matrix products, arithmetic and copies ran while one was open for 4% of the time, Pallas kernels for 0%

profile of v1, /device:TPU:0, one launch (start us, length us, event | category | flops | bytes accessed | tf_op | source)
XLA Modules:
  0.0 286.9 jit_solution(16189830074422669262)
XLA Ops:
  7.2 0.0 copy-start.2
  7.2 0.0 all-gather.9.cloned.1.call-start
  7.2 2.7 convert_element_type.24
  9.9 0.0 all-gather.9.cloned.1.call-update
  10.0 0.0 all-gather.7.cloned.1.call-start
  10.0 1.9 copy.7
  11.9 0.0 copy-done.2
  12.0 0.0 copy-start.1
  12.0 1.1 multiply_convert_fusion.1
  13.0 0.0 all-gather.7.cloned.1.call-update
  13.1 0.0 all-gather.11.cloned.1.call-start
  13.1 10.3 %all-gather.9.cloned.1.call-done = bf16[512,2048]{1,0:T(8,128)(2,1)} async-done(((bf16[512,1024]{1,0:T(8,128)(2,1)}), bf16[512,2048]{1,0:T(8,128)(2,1)}) %all-gather.9.cloned.1.call-update) | async-done | bytes 2097168 | tf_op jit(solution)/shard_map/all_gather | solution.py:23
  23.4 0.0 all-gather.11.cloned.1.call-update
  23.5 0.0 all-gather.5.cloned.1.call-start
  23.5 0.2 fusion
  23.7 1.0 fusion.1
  24.7 0.0 all-gather.5.cloned.1.call-update
  24.7 12.6 %all-gather.7.cloned.1.call-done = bf16[128,8192]{0,1:T(8,128)(2,1)} async-done(((bf16[128,4096]{0,1:T(8,128)(2,1)}), bf16[128,8192]{0,1:T(8,128)(2,1)}) %all-gather.7.cloned.1.call-update) | async-done | bytes 2097168 | tf_op jit(solution)/shard_map/all_gather | solution.py:22
  37.3 1.7 copy.8
  39.1 54.3 %all_to_all.21 = bf16[128,8,1024]{0,2,1:T(8,128)(2,1)} all-to-all(bf16[128,8,1024]{0,2,1:T(8,128)(2,1)S(1)} %bitcast.11), channel_id=1, replica_groups=mesh['gr'=2,'fs'=8,'tp'=2] {'fs'}, dimensions={1} | all-to-all | bytes 4194304 | tf_op jit(solution)/shard_map/all_to_all | solution.py:31
  93.4 2.9 copy.9
  96.3 2.4 pad_maximum_fusion
  98.7 5.6 %all-to-all-start.1 = ((bf16[2,1024,1024]{2,1,0:T(8,128)(2,1)}), bf16[2,1024,1024]{2,1,0:T(8,128)(2,1)}, u32[]{:S(2)}, u32[]{:S(2)}) async-start(bf16[2,1024,1024]{2,1,0:T(8,128)(2,1)} %pad_maximum_fusion), calls=%async_computation.1 | async-start | bytes 8388608 | tf_op jit(solution)/shard_map/all_to_all | solution.py:10
  104.3 0.0 reduce-scatter.2.cloned.1.call-start
  104.4 0.0 all-gather.11.cloned.1.call-done
  104.4 67.8 %all-gather.5.cloned.1.call-done = bf16[1024,2048]{1,0:T(8,128)(2,1)} async-done(((bf16[128,2048]{1,0:T(8,128)(2,1)}), bf16[1024,2048]{1,0:T(8,128)(2,1)}) %all-gather.5.cloned.1.call-update) | async-done | bytes 4194320 | tf_op jit(solution)/shard_map/all_gather | solution.py:41
  172.2 0.0 all-to-all-done.1
  172.2 14.4 %convolution_convert_fusion = bf16[1024,2048]{1,0:T(8,128)(2,1)} fusion(bf16[1024,2048]{1,0:T(8,128)(2,1)} %all-gather.11.cloned.1.call-done, bf16[1024,2048]{1,0:T(8,128)(2,1)} %all-gather.5.cloned.1.call-done, bf16[2048,1024]{1,0:T(8,128)(2,1)} %bitcast.5), kind=kOutput, calls=%fused_computation.2 | convolution fusion | flops 8595177472 | bytes 16777216 | tf_op jit(solution)/shard_map/dot_general | solution.py:46
  186.6 0.0 reduce-scatter.2.cloned.1.call-update
  186.6 87.0 %reduce-scatter.2.cloned.1.call-done = bf16[128,2048]{1,0:T(8,128)(2,1)} async-done(((bf16[1024,2048]{1,0:T(8,128)(2,1)}), bf16[128,2048]{1,0:T(8,128)(2,1)}) %reduce-scatter.2.cloned.1.call-update) | async-done | bytes 524304 | tf_op jit(solution)/shard_map/reduce_scatter | solution.py:48
  273.6 4.8 %copy.12 = bf16[2048,1024]{1,0:T(8,128)(2,1)} copy(bf16[2048,1024]{1,0:T(8,128)(2,1)} %bitcast.5) | data formatting | bytes 8388608
  278.4 2.0 copy.13
  (4 shorter events, 0.0 us)
Async XLA Ops:
  7.2 4.8 %copy-start.2 = (f32[128]{0:T(128)S(1)}, f32[128]{0:T(128)}, u32[]{:S(2)}) copy-start(f32[128]{0:T(128)} %param.5) | copy-start | bytes 1540
  7.2 16.3 %all-gather.9.cloned.1.call-start = ((), (), s32[]{:S(2)}) async-start(), calls=%async_computation.5 | async-start | bytes 3145728 | tf_op jit(solution)/shard_map/all_gather | solution.py:23
  10.0 27.4 %all-gather.7.cloned.1.call-start = ((), (), s32[]{:S(2)}) async-start(), calls=%async_computation.4 | async-start | bytes 3145728 | tf_op jit(solution)/shard_map/all_gather | solution.py:22
  12.0 11.6 %copy-start.1 = (bf16[128,2048]{1,0:T(8,128)(2,1)S(1)}, bf16[128,2048]{1,0:T(8,128)(2,1)}, u32[]{:S(2)}) copy-start(bf16[128,2048]{1,0:T(8,128)(2,1)} %param.4) | copy-start | bytes 1572868
  13.1 91.3 %all-gather.11.cloned.1.call-start = ((), (), s32[]{:S(2)}) async-start(), calls=%async_computation.6 | async-start | bytes 6291456 | tf_op jit(solution)/shard_map/all_gather | solution.py:34
  23.5 148.7 %all-gather.5.cloned.1.call-start = ((), (), s32[]{:S(2)}) async-start(), calls=%async_computation.3 | async-start | bytes 4718592 | tf_op jit(solution)/shard_map/all_gather | solution.py:41
  98.7 73.5 %all-to-all-start.1 = ((bf16[2,1024,1024]{2,1,0:T(8,128)(2,1)}), bf16[2,1024,1024]{2,1,0:T(8,128)(2,1)}, u32[]{:S(2)}, u32[]{:S(2)}) async-start(bf16[2,1024,1024]{2,1,0:T(8,128)(2,1)} %pad_maximum_fusion), calls=%async_computation.1 | async-start | bytes 8388608 | tf_op jit(solution)/shard_map/all_to_all | solution.py:10
  104.3 169.3 %reduce-scatter.2.cloned.1.call-start = ((), (), s32[]{:S(2)}) async-start(), calls=%async_computation.7 | async-start | bytes 4718592 | tf_op jit(solution)/shard_map/reduce_scatter | solution.py:48
  273.6 4.8 %copy-start = (bf16[1024,2048]{1,0:T(8,128)(2,1)S(1)}, bf16[1024,2048]{1,0:T(8,128)(2,1)}, u32[]{:S(2)}) copy-start(bf16[1024,2048]{1,0:T(8,128)(2,1)} %all-gather.11.cloned.1.call-done) | copy-start | bytes 12582916
Sparse Core Ops, SparseCore 0:
  10.1 13.2 all-gather.8
  25.5 11.7 all-gather.6
  38.9 57.8 all-gather.10
  99.4 72.7 all-gather.4
  186.7 86.8 reduce-scatter.1
